TPU v7x, 32 devices: a whole 2x2x4 slice. The times are simulated.
32 devices in a mesh: ep: 8 (over z, core), tp: 4 (over y, x).
Axes of the slice: x: 2, y: 2, z: 4, core: 2. Of those that a mesh axis runs over, the one named last changes fastest.
Arguments:
- tokens: bfloat16 [256, 4096], P('ep'), may hold values from -6 to 6
- recur_state: float32 [256, 4096], P('ep', 'tp'), may hold values from -6 to 6
- conv_state: bfloat16 [256, 3, 4096], P('ep', None, 'tp'), may hold values from -6 to 6
- mix_gain: float32 [4096], replicated, may hold values from 0.1 to 1.9
- in_weight: bfloat16 [4096, 4096], P('ep', 'tp'), may hold values from -0.09375 to 0.09375
- gate_weight: bfloat16 [4096, 4096], P('ep', 'tp'), may hold values from -0.09375 to 0.09375
- conv_taps: float32 [4, 4096], P(None, 'tp'), may hold values from -3 to 3
- recur_gate_blocks: bfloat16 [64, 64, 64], P('tp'), may hold values from -0.75 to 0.75
- input_gate_blocks: bfloat16 [64, 64, 64], P('tp'), may hold values from -0.75 to 0.75
- decay_rate: float32 [4096], P('tp'), may hold values from 0.01 to 0.4
- out_weight: bfloat16 [4096, 4096], P('tp', 'ep'), may hold values from -0.09375 to 0.09375
- ffn_gain: float32 [4096], replicated, may hold values from 0.1 to 1.9
- router_weight: bfloat16 [4096, 8], replicated, may hold values from -0.09375 to 0.09375
- routes: int32 [256, 2], P('ep'), may hold values from 0 to 7, as said below
- expert_gate: bfloat16 [8, 4096, 2048], P('ep', None, 'tp'), may hold values from -0.09375 to 0.09375
- expert_up: bfloat16 [8, 4096, 2048], P('ep', None, 'tp'), may hold values from -0.09375 to 0.09375
- expert_down: bfloat16 [8, 2048, 4096], P('ep', 'tp'), may hold values from -0.125 to 0.125
- dense_gate: bfloat16 [4096, 2048], P('ep', 'tp'), may hold values from -0.09375 to 0.09375
- dense_up: bfloat16 [4096, 2048], P('ep', 'tp'), may hold values from -0.09375 to 0.09375
- dense_down: bfloat16 [2048, 4096], P('tp', 'ep'), may hold values from -0.125 to 0.125
- branch_gate: bfloat16 [4096], replicated, may hold values from -0.09375 to 0.09375
Outputs:
- layer_out: bfloat16 [256, 4096], P('ep')
- new_state: float32 [256, 4096], P('ep', 'tp')
- new_conv_state: bfloat16 [256, 3, 4096], P('ep', None, 'tp')
Inputs may be any that keep to these rules, and one draw needn't show every extreme that they name: `routes`: A row names two different experts of one group: both have the same e // 4. In the rows of one index of ep no expert is named more than 16 times, and in every draw some expert is named exactly 16 times by the rows of every index of ep.
All inputs are finite; a program needn't handle non-finite values.
Results may differ from a plain program's by a relative error of at most 0.023.
Values may be sent and summed in bfloat16 or wider, within the bound.
A program may use at most 64 MiB of HBM per device.

v0:
```python
import jax
import jax.numpy as jnp
from jax import lax
from jax.sharding import PartitionSpec as P

TOP_K = 2


epsilon = 1e-06
decay_scale = 8.0


def rms_scale(rows, gain):
    values = rows.astype(jnp.float32)
    inverse = lax.rsqrt(jnp.mean(values * values, axis=-1, keepdims=True) + epsilon)
    return (values * inverse * gain).astype(jnp.bfloat16)


def on_device(
    tokens,
    recur_state,
    conv_state,
    mix_gain,
    in_weight,
    gate_weight,
    conv_taps,
    recur_gate_blocks,
    input_gate_blocks,
    decay_rate,
    out_weight,
    ffn_gain,
    router_weight,
    routes,
    expert_gate,
    expert_up,
    expert_down,
    dense_gate,
    dense_up,
    dense_down,
    branch_gate,
):
    batch_rows, width = tokens.shape
    channels = in_weight.shape[1]
    normed = rms_scale(tokens, mix_gain)
    arrived = lax.all_to_all(normed, "ep", split_axis=1, concat_axis=0, tiled=True)
    joined = jnp.concatenate([in_weight, gate_weight], axis=1)
    summed = lax.psum_scatter(
        jnp.dot(arrived, joined, preferred_element_type=jnp.float32).astype(jnp.bfloat16),
        "ep",
        scatter_dimension=0,
        tiled=True,
    ).astype(jnp.float32)
    x_sum, gate_sum = (summed[:, :channels], summed[:, channels:])
    x_branch = x_sum.astype(jnp.bfloat16)
    gate_branch = gate_sum.astype(jnp.bfloat16)
    window = jnp.concatenate([conv_state, x_branch[:, None, :]], axis=1)
    conv_out = jnp.sum(window.astype(jnp.float32) * conv_taps[None], axis=1).astype(jnp.bfloat16)
    new_conv_state = window[:, 1:, :]
    blocks = conv_out.reshape(batch_rows, recur_gate_blocks.shape[0], recur_gate_blocks.shape[1])
    recur_gate = jax.nn.sigmoid(
        jnp.einsum(
            "bhi,hij->bhj", blocks, recur_gate_blocks, preferred_element_type=jnp.float32
        ).reshape(batch_rows, channels)
    )
    input_gate = jax.nn.sigmoid(
        jnp.einsum(
            "bhi,hij->bhj", blocks, input_gate_blocks, preferred_element_type=jnp.float32
        ).reshape(batch_rows, channels)
    )
    log_decay = -decay_scale * recur_gate * decay_rate
    new_state = jnp.exp(log_decay) * recur_state + jnp.sqrt(
        -jnp.expm1(2.0 * log_decay)
    ) * input_gate * conv_out.astype(jnp.float32)
    mixer_rows = (new_state * jax.nn.gelu(gate_branch.astype(jnp.float32))).astype(jnp.bfloat16)
    mixer_part = jnp.dot(
        mixer_rows,
        lax.all_gather(out_weight, "ep", axis=1, tiled=True),
        preferred_element_type=jnp.float32,
    )
    resid = (
        tokens.astype(jnp.float32)
        + lax.psum(mixer_part.astype(jnp.bfloat16), "tp").astype(jnp.float32)
    ).astype(jnp.bfloat16)
    normed_ffn = rms_scale(resid, ffn_gain)
    router_logits = jnp.dot(normed_ffn, router_weight, preferred_element_type=jnp.float32)
    experts = router_logits.shape[1]
    expert_ids = lax.broadcasted_iota(jnp.int32, (batch_rows, TOP_K, experts), 2)
    picked = jnp.sum(
        jnp.where(routes[:, :, None] == expert_ids, router_logits[:, None, :], 0.0), axis=2
    )
    route_weight = jax.nn.sigmoid(picked - picked[:, ::-1]).astype(jnp.bfloat16)
    capacity = 2 * batch_rows * TOP_K // experts
    flat_ids = routes.reshape(batch_rows * TOP_K)
    onehot = (
        flat_ids[:, None] == lax.broadcasted_iota(jnp.int32, (batch_rows * TOP_K, experts), 1)
    ).astype(jnp.int32)
    rank = jnp.sum((jnp.cumsum(onehot, axis=0) - onehot) * onehot, axis=1)
    slot_of = (flat_ids * capacity + rank).reshape(batch_rows, TOP_K)
    slot_rows = lax.broadcasted_iota(jnp.int32, (experts * capacity, batch_rows), 0)
    slot_cols = lax.broadcasted_iota(jnp.int32, (batch_rows, experts * capacity), 1)
    dispatch = jnp.zeros((experts * capacity, batch_rows), jnp.bfloat16)
    combine = jnp.zeros((batch_rows, experts * capacity), jnp.bfloat16)
    for pick in range(TOP_K):
        dispatch = dispatch + (slot_rows == slot_of[None, :, pick]).astype(jnp.bfloat16)
        combine = combine + jnp.where(
            slot_cols == slot_of[:, pick : pick + 1],
            route_weight[:, pick : pick + 1],
            jnp.zeros((), jnp.bfloat16),
        )
    outgoing = (
        jnp.dot(dispatch, normed_ffn, preferred_element_type=jnp.float32)
        .astype(jnp.bfloat16)
        .reshape(experts, capacity, width)
    )
    gate_local = expert_gate[0]
    up_local = expert_up[0]
    down_local = expert_down[0]
    arrived_rows = lax.all_to_all(outgoing, "ep", split_axis=0, concat_axis=0, tiled=True)
    sources, items, features = arrived_rows.shape
    rows = arrived_rows.reshape(sources * items, features)
    first = jnp.dot(rows, gate_local, preferred_element_type=jnp.float32)
    second = jnp.dot(rows, up_local, preferred_element_type=jnp.float32)
    act = (jax.nn.silu(first) * second).astype(jnp.bfloat16)
    partial_value = jnp.dot(act, down_local, preferred_element_type=jnp.float32)
    total = lax.psum(partial_value.astype(jnp.bfloat16), "tp")
    returned = lax.all_to_all(
        total.reshape(sources, items, total.shape[1]), "ep", split_axis=0, concat_axis=0, tiled=True
    )
    moe = jnp.dot(
        combine,
        returned.reshape(experts * capacity, returned.shape[2]),
        preferred_element_type=jnp.float32,
    )
    dense_arrived = lax.all_to_all(normed_ffn, "ep", split_axis=1, concat_axis=0, tiled=True)
    dense_joined = jnp.concatenate([dense_gate, dense_up], axis=1)
    dense_summed = lax.psum_scatter(
        jnp.dot(dense_arrived, dense_joined, preferred_element_type=jnp.float32).astype(
            jnp.bfloat16
        ),
        "ep",
        scatter_dimension=0,
        tiled=True,
    ).astype(jnp.float32)
    dense_first = dense_summed[:, : dense_gate.shape[1]]
    dense_second = dense_summed[:, dense_gate.shape[1] :]
    dense_act = (jax.nn.silu(dense_first) * dense_second).astype(jnp.bfloat16)
    dense_part = jnp.dot(
        dense_act,
        lax.all_gather(dense_down, "ep", axis=1, tiled=True),
        preferred_element_type=jnp.float32,
    )
    branch_weight = jax.nn.sigmoid(
        jnp.dot(normed_ffn, branch_gate, preferred_element_type=jnp.float32)
    )
    dense_sum = lax.psum(dense_part.astype(jnp.bfloat16), "tp").astype(jnp.float32)
    layer_out = (resid.astype(jnp.float32) + moe + branch_weight[:, None] * dense_sum).astype(
        jnp.bfloat16
    )
    return (layer_out, new_state, new_conv_state)


def solution(mesh):
    in_specs = (
        P("ep", None),
        P("ep", "tp"),
        P("ep", None, "tp"),
        P(),
        P("ep", "tp"),
        P("ep", "tp"),
        P(None, "tp"),
        P("tp", None, None),
        P("tp", None, None),
        P("tp"),
        P("tp", "ep"),
        P(),
        P(),
        P("ep", None),
        P("ep", None, "tp"),
        P("ep", None, "tp"),
        P("ep", "tp", None),
        P("ep", "tp"),
        P("ep", "tp"),
        P("tp", "ep"),
        P(),
    )
    out_specs = (P("ep", None), P("ep", "tp"), P("ep", None, "tp"))
    return jax.shard_map(
        on_device, mesh=mesh, in_specs=in_specs, out_specs=out_specs, check_vma=False
    )
```

profile of v0, /device:TPU:0, one launch (start us, length us, event | category | flops | bytes accessed | tf_op | source)
XLA Modules:
  0.0 396.9 jit_solution(11186199223250125864)
XLA Ops:
  7.2 1.1 fusion.33
  8.4 1.1 fusion.35
  9.5 16.0 %all_to_all.48 = bf16[32,8,512]{2,0,1:T(8,128)(2,1)S(1)} all-to-all(bf16[32,8,512]{2,0,1:T(8,128)(2,1)S(1)} %bitcast.77), channel_id=1, replica_groups=mesh['ep'=8,'tp'=4] {'ep'}, dimensions={1} | all-to-all | bytes 524288 | tf_op jit(solution)/shard_map/all_to_all | solution.py:45
  25.5 3.4 convolution_convert_fusion.4
  29.0 0.7 all-gather.3.cloned.1.call-update
  29.8 30.9 %reduce-scatter.3.cloned.1.call-done = bf16[32,2048]{1,0:T(8,128)(2,1)} async-done(((bf16[256,2048]{1,0:T(8,128)(2,1)}), bf16[32,2048]{1,0:T(8,128)(2,1)}) %reduce-scatter.3.cloned.1.call-update) | async-done | bytes 131088 | tf_op jit(solution)/shard_map/reduce_scatter | solution.py:47
  60.7 0.9 slice_bitcast_fusion
  61.6 0.1 multiply_reduce_fusion
  61.7 0.1 convert_element_type.92
  61.9 0.2 fusion.17
  62.1 0.2 copy.55
  62.2 0.1 div.34
  62.4 0.2 fusion.13
  62.6 0.2 copy.57
  62.8 0.1 div.36
  62.9 0.1 multiply_add_fusion
  63.1 79.5 %all-gather.3.cloned.1.call-done = bf16[1024,4096]{1,0:T(8,128)(2,1)} async-done(((bf16[1024,512]{1,0:T(8,128)(2,1)}), bf16[1024,4096]{1,0:T(8,128)(2,1)}) %all-gather.3.cloned.1.call-update) | async-done | bytes 8388624 | tf_op jit(solution)/shard_map/all_gather | solution.py:77
  142.5 5.6 %convolution_convert_fusion.3 = bf16[32,4096]{1,0:T(8,128)(2,1)} fusion(bf16[1024,4096]{1,0:T(8,128)(2,1)} %all-gather.3.cloned.1.call-done, f32[32,1024]{1,0:T(8,128)S(1)} %multiply_add_fusion, bf16[32,2048]{1,0:T(8,128)(2,1)S(1)} %copy-done.5), kind=kOutput, calls=%fused_computation.6 | convolution fusion | flops 268926976 | bytes 8847360 | tf_op jit(solution)/shard_map/dot_general | solution.py:75
  148.2 0.0 reduce-scatter.5.cloned.1.call-start
  148.2 41.6 %all-reduce.4.cloned.1.call-done = bf16[32,4096]{1,0:T(8,128)(2,1)} async-done(((bf16[32,4096]{1,0:T(8,128)(2,1)}), bf16[32,4096]{1,0:T(8,128)(2,1)}) %all-reduce.4.cloned.1.call-update) | async-done | bytes 262160 | tf_op jit(solution)/shard_map/psum | solution.py:82
  189.9 1.1 fusion.37
  191.0 1.1 fusion.39
  192.1 14.1 %all_to_all.49 = bf16[32,8,512]{2,0,1:T(8,128)(2,1)S(1)} all-to-all(bf16[32,8,512]{2,0,1:T(8,128)(2,1)S(1)} %bitcast.78), channel_id=1, replica_groups=mesh['ep'=8,'tp'=4] {'ep'}, dimensions={1} | all-to-all | bytes 524288 | tf_op jit(solution)/shard_map/all_to_all | solution.py:134
  206.2 1.3 convolution_convert_fusion.5
  207.6 0.5 all-gather.5.cloned.1.call-update
  208.2 0.1 copy.58
  208.2 0.1 eq.54
  208.4 0.1 fusion.72
  208.4 0.1 reduce_window_sum.11
  208.5 0.2 select_reduce_fusion
  208.7 0.1 reduce_sum.50
  208.8 0.1 copy.59
  208.9 1.4 convolution_convert_fusion.1
  210.3 3.6 all-to-all-start.1
  213.9 0.0 all-reduce.6.cloned.1.call-start
  213.9 24.5 %reduce-scatter.5.cloned.1.call-done = bf16[32,1024]{1,0:T(8,128)(2,1)} async-done(((bf16[256,1024]{1,0:T(8,128)(2,1)}), bf16[32,1024]{1,0:T(8,128)(2,1)}) %reduce-scatter.5.cloned.1.call-update) | async-done | bytes 65552 | tf_op jit(solution)/shard_map/reduce_scatter | solution.py:136
  238.4 0.8 convert_element_type.109
  239.2 49.8 %all-gather.5.cloned.1.call-done = bf16[512,4096]{1,0:T(8,128)(2,1)} async-done(((bf16[512,512]{1,0:T(8,128)(2,1)}), bf16[512,4096]{1,0:T(8,128)(2,1)}) %all-gather.5.cloned.1.call-update) | async-done | bytes 4194320 | tf_op jit(solution)/shard_map/all_gather | solution.py:149
  289.0 3.7 convolution_convert_fusion.2
  292.7 2.9 fusion.5
  295.7 5.9 %convolution_convert_fusion = bf16[128,4096]{1,0:T(8,128)(2,1)} fusion(bf16[1,512,4096]{2,1,0:T(8,128)(2,1)} %param.37, bf16[128,4096]{1,0:T(8,128)(2,1)S(1)} %bitcast.72, bf16[1,4096,512]{2,1,0:T(8,128)(2,1)} %param.36, f32[128,512]{1,0:T(8,128)S(1)} %fusion.5), kind=kOutput, calls=%fused_computation | convolution fusion | flops 1074659328 | bytes 10747904 | tf_op jit(solution)/shard_map/dot_general | solution.py:124
  301.6 55.4 %all-reduce.6.cloned.1.call-done = (bf16[8,16,4096]{2,1,0:T(8,128)(2,1)}, bf16[32,4096]{1,0:T(8,128)(2,1)}) async-done(((bf16[8,16,4096]{2,1,0:T(8,128)(2,1)}, bf16[32,4096]{1,0:T(8,128)(2,1)}), (bf16[8,16,4096]{2,1,0:T(8,128)(2,1)}, bf16[32,4096]{1,0:T(8,128)(2,1)})) %all-reduce.6.cloned.1.call-update) | async-done | bytes 1310736 | tf_op jit(solution)/shard_map/psum | solution.py:125
  356.9 4.6 %all-to-all-start.2 = ((bf16[8,16,4096]{2,1,0:T(8,128)(2,1)}), bf16[8,16,4096]{2,1,0:T(8,128)(2,1)S(1)}, u32[]{:S(2)}, u32[]{:S(2)}) async-start(bf16[8,16,4096]{2,1,0:T(8,128)(2,1)} %get-tuple-element.3), calls=%async_computation.3 | async-start | bytes 2097152 | tf_op jit(solution)/shard_map/all_to_all | solution.py:126
  361.5 0.7 fusion.45
  362.2 0.2 fusion.93
  362.5 0.2 fusion.27
  362.7 25.4 %all-to-all-done.2 = bf16[8,16,4096]{2,1,0:T(8,128)(2,1)S(1)} async-done(((bf16[8,16,4096]{2,1,0:T(8,128)(2,1)}), bf16[8,16,4096]{2,1,0:T(8,128)(2,1)S(1)}, u32[]{:S(2)}, u32[]{:S(2)}) %all-to-all-start.2) | async-done | bytes 1048608 | tf_op jit(solution)/shard_map/all_to_all | solution.py:126
  388.1 2.0 fusion.1
  (53 shorter events, 0.5 us)
Async XLA Ops:
  7.2 54.7 %copy-start = (bf16[16,64,64]{2,1,0:T(8,128)(2,1)S(1)}, bf16[16,64,64]{2,1,0:T(8,128)(2,1)}, u32[]{:S(2)}) copy-start(bf16[16,64,64]{2,1,0:T(8,128)(2,1)} %param.28) | copy-start | bytes 393220
  7.2 53.5 %reduce-scatter.3.cloned.1.call-start = ((), (), s32[]{:S(2)}) async-start(), calls=%async_computation.6 | async-start | bytes 1179648 | tf_op jit(solution)/shard_map/reduce_scatter | solution.py:47
  8.4 21.4 %copy-start.12 = (f32[1024]{0:T(1024)S(1)}, f32[1024]{0:T(1024)}, u32[]{:S(2)}) copy-start(f32[1024]{0:T(1024)} %param.30) | copy-start | bytes 12292
  9.5 52.1 %copy-start.4 = (bf16[32,3,1024]{2,0,1:T(8,128)(2,1)S(1)}, bf16[32,3,1024]{2,0,1:T(8,128)(2,1)}, u32[]{:S(2)}) copy-start(bf16[32,3,1024]{2,0,1:T(8,128)(2,1)} %param.23) | copy-start | bytes 589828
  9.5 52.1 %copy-start.9 = (f32[4,1024]{1,0:T(4,128)S(1)}, f32[4,1024]{1,0:T(4,128)}, u32[]{:S(2)}) copy-start(f32[4,1024]{1,0:T(4,128)} %param.27) | copy-start | bytes 49156
  25.5 36.8 %copy-start.15 = (bf16[16,64,64]{2,1,0:T(8,128)(2,1)S(1)}, bf16[16,64,64]{2,1,0:T(8,128)(2,1)}, u32[]{:S(2)}) copy-start(bf16[16,64,64]{2,1,0:T(8,128)(2,1)} %param.29) | copy-start | bytes 393220
  28.9 34.0 %copy-start.6 = (f32[32,1024]{1,0:T(8,128)S(1)}, f32[32,1024]{1,0:T(8,128)}, u32[]{:S(2)}) copy-start(f32[32,1024]{1,0:T(8,128)} %param.22) | copy-start | bytes 393220
  28.9 113.6 %all-gather.3.cloned.1.call-start = ((), (), s32[]{:S(2)}) async-start(), calls=%async_computation.7 | async-start | bytes 9437184 | tf_op jit(solution)/shard_map/all_gather | solution.py:77
  29.7 160.2 %all-reduce.4.cloned.1.call-start = ((), (), s32[]{:S(2)}) async-start(), calls=%async_computation.8 | async-start | bytes 524288 | tf_op jit(solution)/shard_map/psum | solution.py:82
  60.7 81.8 %copy-start.5 = (bf16[32,2048]{1,0:T(8,128)(2,1)S(1)}, bf16[32,2048]{1,0:T(8,128)(2,1)}, u32[]{:S(2)}) copy-start(bf16[32,2048]{1,0:T(8,128)(2,1)} %reduce-scatter.3.cloned.1.call-done) | copy-start | bytes 393220
  63.0 85.1 %copy-start.3 = (f32[32,1024]{1,0:T(8,128)}, f32[32,1024]{1,0:T(8,128)S(1)}, u32[]{:S(2)}) copy-start(f32[32,1024]{1,0:T(8,128)S(1)} %multiply_add_fusion) | copy-start | bytes 393220
  63.0 126.8 %copy-start.1 = (bf16[32,4096]{1,0:T(8,128)(2,1)S(1)}, bf16[32,4096]{1,0:T(8,128)(2,1)}, u32[]{:S(2)}) copy-start(bf16[32,4096]{1,0:T(8,128)(2,1)} %param.21) | copy-start | bytes 786436
  63.0 128.0 %copy-start.8 = (f32[4096]{0:T(1024)S(1)}, f32[4096]{0:T(1024)}, u32[]{:S(2)}) copy-start(f32[4096]{0:T(1024)} %param.32) | copy-start | bytes 49156
  63.1 143.2 %copy-start.13 = (bf16[512,512]{1,0:T(8,128)(2,1)S(1)}, bf16[512,512]{1,0:T(8,128)(2,1)}, u32[]{:S(2)}) copy-start(bf16[512,512]{1,0:T(8,128)(2,1)} %param.39) | copy-start | bytes 1572868
  63.1 143.2 %copy-start.14 = (bf16[512,512]{1,0:T(8,128)(2,1)S(1)}, bf16[512,512]{1,0:T(8,128)(2,1)}, u32[]{:S(2)}) copy-start(bf16[512,512]{1,0:T(8,128)(2,1)} %param.38) | copy-start | bytes 1572868
  148.2 60.0 %copy-start.10 = (s32[32,2]{0,1:T(2,128)S(1)}, s32[32,2]{0,1:T(2,128)}, u32[]{:S(2)}) copy-start(s32[32,2]{0,1:T(2,128)} %param.34) | copy-start | bytes 772
  148.2 90.2 %reduce-scatter.5.cloned.1.call-start = ((), (), s32[]{:S(2)}) async-start(), calls=%async_computation.9 | async-start | bytes 589824 | tf_op jit(solution)/shard_map/reduce_scatter | solution.py:136
  207.6 81.4 %all-gather.5.cloned.1.call-start = ((), (), s32[]{:S(2)}) async-start(), calls=%async_computation.10 | async-start | bytes 4718592 | tf_op jit(solution)/shard_map/all_gather | solution.py:149
  210.3 82.4 %all-to-all-start.1 = ((bf16[8,16,4096]{2,1,0:T(8,128)(2,1)}), bf16[8,16,4096]{2,1,0:T(8,128)(2,1)S(1)}, u32[]{:S(2)}, u32[]{:S(2)}) async-start(bf16[8,16,4096]{2,1,0:T(8,128)(2,1)} %bitcast.9), calls=%async_computation.2 | async-start | bytes 2097152 | tf_op jit(solution)/shard_map/all_to_all | solution.py:118
  213.9 143.0 %all-reduce.6.cloned.1.call-start = ((), (), s32[]{:S(2)}) async-start(), calls=%async_computation.11 | async-start | bytes 2621440 | tf_op jit(solution)/shard_map/psum | solution.py:125
  295.6 65.9 %copy-start.11 = (bf16[4096]{0:T(1024)(128)(2,1)S(1)}, bf16[4096]{0:T(1024)(128)(2,1)}, u32[]{:S(2)}) copy-start(bf16[4096]{0:T(1024)(128)(2,1)} %param.41) | copy-start | bytes 24580
  295.6 66.6 %copy-start.7 = (bf16[4096,8]{0,1:T(8,128)(2,1)S(1)}, bf16[4096,8]{0,1:T(8,128)(2,1)}, u32[]{:S(2)}) copy-start(bf16[4096,8]{0,1:T(8,128)(2,1)} %param.33) | copy-start | bytes 196612
  301.5 86.5 %copy-start.2 = (bf16[32,4096]{1,0:T(8,128)(2,1)S(1)}, bf16[32,4096]{1,0:T(8,128)(2,1)}, u32[]{:S(2)}) copy-start(bf16[32,4096]{1,0:T(8,128)(2,1)} %all-reduce.4.cloned.1.call-done) | copy-start | bytes 786436
  356.9 31.2 %all-to-all-start.2 = ((bf16[8,16,4096]{2,1,0:T(8,128)(2,1)}), bf16[8,16,4096]{2,1,0:T(8,128)(2,1)S(1)}, u32[]{:S(2)}, u32[]{:S(2)}) async-start(bf16[8,16,4096]{2,1,0:T(8,128)(2,1)} %get-tuple-element.3), calls=%async_computation.3 | async-start | bytes 2097152 | tf_op jit(solution)/shard_map/all_to_all | solution.py:126
Sparse Core Ops, SparseCore 0:
  29.1 31.6 reduce-scatter.2
  62.3 80.1 all-gather.2
  148.3 41.5 all-reduce.3
  207.7 30.6 reduce-scatter.4
  239.8 49.1 all-gather.4
  301.7 55.1 all-reduce.5
where the time goes:
time: 398 us; the launch traced here: 397 us
  waiting for transfers between devices  308 us (77%)
  blocking collectives  30.1 us (8%)
  matrix products  26.9 us (7%)
  between operations  14.4 us (4%)
  starting transfers between devices  8.4 us (2%)
  other arithmetic  6.59 us (2%)
    all_gather x1, waiting for transfers between devices, on_device(): lax.all_gather(out_weight, 'ep', axis=1, tiled=True)  79.5 us
    psum x1, waiting for transfers between devices, on_device(): total = lax.psum(partial_value.astype(jnp.bfloat16), 'tp')  55.4 us
    all_gather x1, waiting for transfers between devices, on_device(): lax.all_gather(dense_down, 'ep', axis=1, tiled=True)  49.8 us
    psum x1, waiting for transfers between devices, on_device(): lax.psum(mixer_part.astype(jnp.bfloat16), 'tp').astype(jnp.float32)  41.6 us
    reduce_scatter x1, waiting for transfers between devices, on_device(): lax.psum_scatter(jnp.dot(arrived, joined, preferred_element_type=jnp.floa...  30.9 us
    all_to_all x1, waiting for transfers between devices, on_device(): lax.all_to_all(total.reshape(sources, items, total.shape[1]), 'ep', split...  25.4 us
    reduce_scatter x1, waiting for transfers between devices, on_device(): lax.psum_scatter(jnp.dot(dense_arrived, dense_joined, preferred_element_t...  24.5 us
    all_to_all x1, blocking collectives, on_device(): lax.all_to_all(normed, 'ep', split_axis=1, concat_axis=0, tiled=True)  16 us
  transfers between devices with their start and end apart: 8, of which 7 were waited for; matrix products, arithmetic and copies ran while one was open for 3% of the time, Pallas kernels for 0%

commit v1 on v0

--- a/solution.py
+++ b/solution.py
@@ -1,9 +1,16 @@
+import functools
+
 import jax
 import jax.numpy as jnp
 from jax import lax
+from jax.experimental import pallas as pl
+from jax.experimental.pallas import tpu as pltpu
 from jax.sharding import PartitionSpec as P
 
 TOP_K = 2
+LANES = 128
+F32 = jnp.float32
+BF16 = jnp.bfloat16
 
 
 epsilon = 1e-06
@@ -159,6 +166,476 @@
     return (layer_out, new_state, new_conv_state)
 
 
+def rcopy(src, dst, send, recv, ep, tp):
+    return pltpu.make_async_remote_copy(
+        src_ref=src,
+        dst_ref=dst,
+        send_sem=send,
+        recv_sem=recv,
+        device_id={"ep": ep, "tp": tp},
+        device_id_type=pl.DeviceIdType.MESH,
+    )
+
+
+def greet(peers):
+    barrier = pltpu.get_barrier_semaphore()
+    for ep, tp in peers:
+        pl.semaphore_signal(
+            barrier, inc=1, device_id={"ep": ep, "tp": tp}, device_id_type=pl.DeviceIdType.MESH
+        )
+    pl.semaphore_wait(barrier, len(peers))
+
+
+def dot(left, right):
+    return jnp.dot(left, right, preferred_element_type=F32)
+
+
+def split_sum(me, tp, zs, half, psend, precv, keep, rsend, rrecv, s2, r2, s3, r3, part, between):
+    z, c = me // 2, me % 2
+    mate = 2 * z + 1 - c
+    sends = []
+    for zz in range(zs):
+        psend[zz] = part(zz, 1 - c)
+        cp = rcopy(psend.at[zz], precv.at[zz], s2.at[zz], r2.at[zz], mate, tp)
+        cp.start()
+        sends.append(cp)
+    for zz in range(zs):
+        keep[zz] = part(zz, c).astype(F32)
+    between()
+    for dz in range(1, zs):
+        zz = lax.rem(z + dz, zs)
+        rcopy(psend.at[zz], precv.at[zz], s2.at[zz], r2.at[zz], mate, tp).wait_recv()
+        rsend[zz] = (keep[zz] + precv[zz].astype(F32)).astype(BF16)
+        cp = rcopy(rsend.at[zz], rrecv.at[z], s3.at[dz], r3.at[dz], 2 * zz + c, tp)
+        cp.start()
+        sends.append(cp)
+    rcopy(psend.at[z], precv.at[z], s2.at[z], r2.at[z], mate, tp).wait_recv()
+
+    def finish():
+        total = keep[z] + precv[z].astype(F32)
+        for dz in range(1, zs):
+            frm = lax.rem(z - dz + zs, zs)
+            rcopy(rrecv.at[frm], rrecv.at[frm], s3.at[dz], r3.at[dz], mate, tp).wait_recv()
+            total += rrecv[frm].astype(F32)
+        return total
+
+    return sends, finish
+
+
+def project_kernel(
+    n, tokens, gain, iw, gw, out, nsend, narr, psend, precv, keep, rsend, rrecv, s1, r1, s2, r2, s3, r3
+):
+    me, tp = lax.axis_index("ep"), lax.axis_index("tp")
+    zs = n // 2
+    q, ch = iw.shape
+    greet([(lax.rem(me + d, n), tp) for d in range(1, n)])
+    values = tokens[...].astype(F32)
+    inverse = lax.rsqrt(jnp.mean(values * values, axis=-1, keepdims=True) + epsilon)
+    normed = (values * inverse * gain[...]).astype(BF16)
+    for e in range(n):
+        nsend[e] = normed[:, e * q : (e + 1) * q]
+    sends = []
+    for d in range(1, n):
+        to = lax.rem(me + d, n)
+        cp = rcopy(nsend.at[to], narr.at[me], s1.at[d], r1.at[d], to, tp)
+        cp.start()
+        sends.append(cp)
+    narr[me] = nsend[me]
+    for d in range(1, n):
+        frm = lax.rem(me - d + n, n)
+        rcopy(narr.at[frm], narr.at[frm], s1.at[d], r1.at[d], frm, tp).wait_recv()
+
+    def part(zz, core):
+        rows = narr[2 * zz + core]
+        return jnp.concatenate([dot(rows, iw[...]), dot(rows, gw[...])], axis=1).astype(psend.dtype)
+
+    more, finish = split_sum(
+        me, tp, zs, None, psend, precv, keep, rsend, rrecv, s2, r2, s3, r3, part, lambda: None
+    )
+    out[...] = finish().astype(BF16)
+    for cp in sends + more:
+        cp.wait_send()
+
+
+def project(n, tokens, gain, iw, gw):
+    rows, width = tokens.shape
+    q, ch = iw.shape
+    zs = n // 2
+    vm = pl.BlockSpec(memory_space=pltpu.VMEM)
+    dma = pltpu.SemaphoreType.DMA
+    return pl.pallas_call(
+        functools.partial(project_kernel, n),
+        out_shape=jax.ShapeDtypeStruct((rows, 2 * ch), BF16),
+        in_specs=[vm] * 4,
+        out_specs=vm,
+        scratch_shapes=[
+            pltpu.VMEM((n, rows, q), BF16),
+            pltpu.VMEM((n, rows, q), BF16),
+            pltpu.VMEM((zs, rows, 2 * ch), BF16),
+            pltpu.VMEM((zs, rows, 2 * ch), BF16),
+            pltpu.VMEM((zs, rows, 2 * ch), F32),
+            pltpu.VMEM((zs, rows, 2 * ch), BF16),
+            pltpu.VMEM((zs, rows, 2 * ch), BF16),
+            dma((n,)),
+            dma((n,)),
+            dma((zs,)),
+            dma((zs,)),
+            dma((zs,)),
+            dma((zs,)),
+        ],
+        compiler_params=pltpu.CompilerParams(
+            collective_id=0, has_side_effects=True, vmem_limit_bytes=40 * 1024 * 1024
+        ),
+        name="project",
+    )(tokens, gain, iw, gw)
+
+
+def layer_kernel(
+    n, m, experts, mr, ow, tokens, gain, mask, rb, dg, du, dd, eg, eu, ed, out,
+    wg, wu, wd, mall, masks, osend, orecv, full, nf, accg, accu, act,
+    psend, precv, dkeep, rsend, rrecv, dact, dall,
+    ysend, yrecv, keep, xsend, xrecv, zsend, zrecv, fblk, fin,
+    lw, ks, kr, as_, ar, bs, br, os_, or_, zs_, zr, xs, xr, ms, mrv,
+    s2, r2, s3, r3, cs, cr, es, er, ys, yr, hs, hr, gs, gr, fs, fr,
+):
+    me, tp = lax.axis_index("ep"), lax.axis_index("tp")
+    zs = n // 2
+    z, c = me // 2, me % 2
+    mate = 2 * z + 1 - c
+    rows, width = tokens.shape
+    q = ow.shape[1]
+    g = q // m
+    everyone = [
+        (lax.rem(me + de, n), lax.rem(tp + dt, m))
+        for de in range(n)
+        for dt in range(m)
+        if de or dt
+    ]
+    loads = [
+        pltpu.make_async_copy(eg, wg, lw.at[n]),
+        pltpu.make_async_copy(eu, wu, lw.at[n + 1]),
+    ] + [
+        pltpu.make_async_copy(ed.at[:, pl.ds(i * q, q)], wd.at[i], lw.at[i]) for i in range(n)
+    ]
+    for cp in loads:
+        cp.start()
+    greet(everyone)
+    sends = []
+
+    def send(*args):
+        cp = rcopy(*args)
+        cp.start()
+        sends.append(cp)
+
+    def arrive(buf, sem):
+        rcopy(buf, buf, sem, sem, mate, tp).wait_recv()
+
+    def zpeer(dz):
+        return lax.rem(z + dz, zs)
+
+    def zfrom(dz):
+        return lax.rem(z - dz + zs, zs)
+
+    def tto(dt):
+        return lax.rem(tp + dt, m)
+
+    def tfrom(dt):
+        return lax.rem(tp - dt + m, m)
+
+    def gather(own, buf, s_a, r_a, s_b, r_b):
+        for dz in range(1, zs):
+            send(own, buf.at[me], s_a.at[dz], r_a.at[dz], 2 * zpeer(dz) + c, tp)
+        send(own, buf.at[me], s_b.at[0], r_b.at[0], mate, tp)
+        buf[me] = own[...]
+        for dz in range(1, zs):
+            slot = 2 * zfrom(dz) + c
+            arrive(buf.at[slot], r_a.at[dz])
+            send(buf.at[slot], buf.at[slot], s_b.at[dz], r_b.at[dz], mate, tp)
+
+    def gathered(buf, r_b):
+        for dz in range(zs):
+            arrive(buf.at[2 * zfrom(dz) + 1 - c], r_b.at[dz])
+
+    gather(mr, mall, as_, ar, bs, br)
+    gathered(mall, br)
+    mixed = dot(mall[...].reshape(n * rows, mr.shape[1]), ow[...]).astype(BF16)
+    for r in range(n):
+        for t in range(m):
+            osend[r, t] = mixed[r * rows : (r + 1) * rows, t * g : (t + 1) * g]
+    for de in range(n):
+        for dt in range(m):
+            if de or dt:
+                r, t = lax.rem(me + de, n), tto(dt)
+                k = de * m + dt
+                send(osend.at[r, t], orecv.at[tp, me], os_.at[k], or_.at[k], r, t)
+    orecv[tp, me] = osend[me, tp]
+    for d in range(1, n):
+        to = lax.rem(me + d, n)
+        send(mask, masks.at[me], ks.at[d], kr.at[d], to, tp)
+    masks[me] = mask[...]
+    for de in range(n):
+        for dt in range(m):
+            if de or dt:
+                k = de * m + dt
+                arrive(orecv.at[tfrom(dt), lax.rem(me - de + n, n)], or_.at[k])
+    for e in range(n):
+        total = orecv[0, e].astype(F32)
+        for t in range(1, m):
+            total += orecv[t, e].astype(F32)
+        own = tokens[:, pl.ds(pl.multiple_of(e * q + tp * g, LANES), g)].astype(F32)
+        full[tp, me, e] = (own + total).astype(BF16)
+
+    def spread(slot, dz):
+        for dt in range(1, m):
+            k = dz * m + dt
+            send(full.at[tp, slot], full.at[tp, slot], xs.at[k], xr.at[k], 2 * z + c, tto(dt))
+        k = dz * m
+        send(full.at[tp, slot], full.at[tp, slot], ms.at[k], mrv.at[k], mate, tp)
+
+    for dz in range(1, zs):
+        send(full.at[tp, me], full.at[tp, me], zs_.at[dz], zr.at[dz], 2 * zpeer(dz) + c, tp)
+    spread(me, 0)
+    for dz in range(1, zs):
+        slot = 2 * zfrom(dz) + c
+        arrive(full.at[tp, slot], zr.at[dz])
+        spread(slot, dz)
+    for dz in range(zs):
+        slot = 2 * zfrom(dz) + c
+        for dt in range(1, m):
+            k = dz * m + dt
+            arrive(full.at[tfrom(dt), slot], xr.at[k])
+            send(
+                full.at[tfrom(dt), slot], full.at[tfrom(dt), slot], ms.at[k], mrv.at[k], mate, tp
+            )
+    for dz in range(zs):
+        slot = 2 * zfrom(dz) + 1 - c
+        for dt in range(m):
+            arrive(full.at[tfrom(dt), slot], mrv.at[dz * m + dt])
+
+    @pl.loop(0, n)
+    def _(r):
+        square = jnp.zeros((rows, g), F32)
+        for t in range(m):
+            for e in range(n):
+                v = full[t, r, e].astype(F32)
+                square += v * v
+        inverse = lax.rsqrt(jnp.sum(square, axis=-1, keepdims=True) / width + epsilon)
+        for t in range(m):
+            for e in range(n):
+                at = e * q + t * g
+                nf[e, r, :, t * g : (t + 1) * g] = (
+                    full[t, r, e].astype(F32) * inverse * gain[:, at : at + g]
+                ).astype(BF16)
+
+    def expert_in(first, last):
+        @pl.loop(first, last)
+        def _(k):
+            x = nf[k].reshape(n * rows, q)
+            accg[...] += dot(x, wg[k])
+            accu[...] += dot(x, wu[k])
+
+    def dpart(zz, core):
+        x = nf[me, 2 * zz + core]
+        return jnp.concatenate([dot(x, dg[...]), dot(x, du[...])], axis=1).astype(BF16)
+
+    def between():
+        accg[...] = jnp.zeros_like(accg)
+        accu[...] = jnp.zeros_like(accu)
+        loads[0].wait()
+        loads[1].wait()
+        expert_in(0, n // 4)
+
+    more, finish = split_sum(
+        me, tp, zs, None, psend, precv, dkeep, rsend, rrecv, s2, r2, s3, r3, dpart, between
+    )
+    sends += more
+    expert_in(n // 4, n)
+    gate = accg[...]
+    act[...] = (gate * jax.nn.sigmoid(gate) * accu[...]).astype(BF16)
+    h = dg.shape[1]
+    both = finish()
+    first = both[:, :h]
+    dact[...] = (first * jax.nn.sigmoid(first) * both[:, h:]).astype(BF16)
+    for dz in range(1, zs):
+        send(dact, dall.at[me], cs.at[dz], cr.at[dz], 2 * zpeer(dz) + c, tp)
+    send(dact, dall.at[me], es.at[0], er.at[0], mate, tp)
+    dall[me] = dact[...]
+
+    logits = dot(nf[0].reshape(n * rows, q), rb[0])
+    for k in range(1, n):
+        logits += dot(nf[k].reshape(n * rows, q), rb[k])
+    for d in range(1, n):
+        arrive(masks.at[lax.rem(me - d + n, n)], kr.at[d])
+    chosen = masks[...].reshape(n * rows, LANES).astype(F32)
+    named = logits * chosen
+    other = jnp.sum(named, axis=-1, keepdims=True) - named
+    weight = (jax.nn.sigmoid(logits - other) * chosen).astype(BF16).astype(F32)
+    lane = lax.broadcasted_iota(jnp.int32, (n * rows, LANES), 1)
+    weight = jnp.sum(jnp.where(lane == me, weight, 0.0), axis=-1, keepdims=True)
+    branch = jnp.sum(
+        jnp.where(lane == experts, jax.nn.sigmoid(logits), 0.0), axis=-1, keepdims=True
+    )
+
+    for cp in loads[2:]:
+        cp.wait()
+    order = [lax.rem(z + 1 + i, m) for i in range(m)]
+    for i in range(m):
+        y = dot(act[...], wd[2 * order[i] + 1 - c]) * weight
+        ysend[i] = y.astype(BF16)
+        send(ysend.at[i], yrecv.at[i], ys.at[i], yr.at[i], mate, tp)
+    for i in range(m):
+        keep[i] = dot(act[...], wd[2 * order[i] + c]) * weight
+    for dz in range(1, zs):
+        slot = 2 * zfrom(dz) + c
+        arrive(dall.at[slot], cr.at[dz])
+        send(dall.at[slot], dall.at[slot], es.at[dz], er.at[dz], mate, tp)
+
+    def forward(i):
+        arrive(yrecv.at[i], yr.at[i])
+        keep[i] = keep[i] + yrecv[i].astype(F32)
+
+        @pl.when(order[i] != tp)
+        def _():
+            dt = lax.rem(order[i] - tp + m, m)
+            xsend[i] = keep[i].astype(BF16)
+            rcopy(
+                xsend.at[i], xrecv.at[dt], hs.at[dt], hr.at[dt], me, order[i]
+            ).start()
+
+    for i in range(m - 1):
+        forward(i)
+    for dz in range(zs):
+        arrive(dall.at[2 * zfrom(dz) + 1 - c], er.at[dz])
+    keep[m - 1] = keep[m - 1] + dot(dall[...].reshape(n * rows, h), dd[...]) * branch
+    forward(m - 1)
+
+    mine = lax.rem(tp - z - 1 + 2 * m, m)
+    total = keep[mine]
+    for dt in range(1, m):
+        arrive(xrecv.at[dt], hr.at[dt])
+        total += xrecv[dt].astype(F32)
+    keep[mine] = total
+    for zz in range(zs):
+        zsend[zz] = total[2 * zz * rows : 2 * (zz + 1) * rows].astype(BF16)
+    for dz in range(1, zs):
+        send(zsend.at[zpeer(dz)], zrecv.at[z], gs.at[dz], gr.at[dz], 2 * zpeer(dz) + c, tp)
+    at = pl.multiple_of(2 * z * rows, rows)
+    total = keep[mine, pl.ds(at, 2 * rows), :]
+    for dz in range(1, zs):
+        arrive(zrecv.at[zfrom(dz)], gr.at[dz])
+        total += zrecv[zfrom(dz)].astype(F32)
+    chunk = 2 * tp + c
+    for core in range(2):
+        resid = jnp.concatenate([full[t, 2 * z + core, chunk] for t in range(m)], axis=1)
+        fblk[core] = (resid.astype(F32) + total[core * rows : (core + 1) * rows]).astype(BF16)
+    for dc in range(2):
+        for dt in range(m):
+            if dc or dt:
+                core = lax.rem(c + dc, 2)
+                k = dc * m + dt
+                send(fblk.at[core], fin.at[chunk], fs.at[k], fr.at[k], 2 * z + core, tto(dt))
+    fin[chunk] = fblk[c]
+    for dc in range(2):
+        for dt in range(m):
+            if dc or dt:
+                k = dc * m + dt
+                arrive(fin.at[2 * tfrom(dt) + lax.rem(c + dc, 2)], fr.at[k])
+    for e in range(n):
+        out[:, e * q : (e + 1) * q] = fin[e]
+    for cp in sends:
+        cp.wait_send()
+    for dt in range(1, m):
+        rcopy(xrecv.at[dt], xrecv.at[dt], hs.at[dt], hr.at[dt], mate, tp).wait_send()
+
+
+def rest(n, m, experts, mr, ow, tokens, gain, mask, rb, dg, du, dd, eg, eu, ed):
+    rows, width = tokens.shape
+    ch, q = ow.shape
+    h, f = dg.shape[1], ed.shape[0]
+    g, zs, b = q // m, n // 2, n * rows
+    vm = pl.BlockSpec(memory_space=pltpu.VMEM)
+    hbm = pl.BlockSpec(memory_space=pl.ANY)
+    v = pltpu.VMEM
+
+    def pairs(*counts):
+        return [pltpu.SemaphoreType.DMA((k,)) for k in counts for _ in range(2)]
+
+    return pl.pallas_call(
+        functools.partial(layer_kernel, n, m, experts),
+        out_shape=jax.ShapeDtypeStruct((rows, width), BF16),
+        in_specs=[vm] * 9 + [hbm] * 3,
+        out_specs=vm,
+        scratch_shapes=[
+            v((n, q, f), BF16), v((n, q, f), BF16), v((n, f, q), BF16),
+            v((n, rows, ch), BF16), v((n, rows, LANES), BF16),
+            v((n, m, rows, g), BF16), v((m, n, rows, g), BF16),
+            v((m, n, n, rows, g), BF16), v((n, n, rows, q), BF16),
+            v((b, f), F32), v((b, f), F32), v((b, f), BF16),
+            v((zs, rows, 2 * h), BF16), v((zs, rows, 2 * h), BF16), v((zs, rows, 2 * h), F32),
+            v((zs, rows, 2 * h), BF16), v((zs, rows, 2 * h), BF16),
+            v((rows, h), BF16), v((n, rows, h), BF16),
+            v((m, b, q), BF16), v((m, b, q), BF16), v((m, b, q), F32),
+            v((m, b, q), BF16), v((m, b, q), BF16),
+            v((zs, 2 * rows, q), BF16), v((zs, 2 * rows, q), BF16),
+            v((2, rows, q), BF16), v((n, rows, q), BF16),
+            pltpu.SemaphoreType.DMA((n + 2,)),
+        ] + pairs(n, zs, zs, n * m, zs, zs * m, zs * m, zs, zs, zs, zs, m, m, zs, 2 * m),
+        compiler_params=pltpu.CompilerParams(
+            collective_id=1, has_side_effects=True, vmem_limit_bytes=58 * 1024 * 1024
+        ),
+        name="rest",
+    )(mr, ow, tokens, gain, mask, rb, dg, du, dd, eg, eu, ed)
+
+
+def in_kernels(
+    n, m, tokens, recur_state, conv_state, mix_gain, in_weight, gate_weight, conv_taps,
+    recur_gate_blocks, input_gate_blocks, decay_rate, out_weight, ffn_gain, router_weight, routes,
+    expert_gate, expert_up, expert_down, dense_gate, dense_up, dense_down, branch_gate,
+):
+    batch_rows, width = tokens.shape
+    channels = in_weight.shape[1]
+    experts = router_weight.shape[1]
+    q = width // n
+    lanes = lax.broadcasted_iota(jnp.int32, (batch_rows, LANES), 1)
+    mask = ((routes[:, 0:1] == lanes) | (routes[:, 1:2] == lanes)).astype(BF16)
+    maps = jnp.concatenate(
+        [
+            router_weight,
+            branch_gate[:, None],
+            jnp.zeros((width, LANES - experts - 1), BF16),
+        ],
+        axis=1,
+    ).reshape(n, q, LANES)
+    summed = project(n, tokens, mix_gain[None, :], in_weight, gate_weight)
+    x_branch, gate_branch = summed[:, :channels], summed[:, channels:]
+    window = jnp.concatenate([conv_state, x_branch[:, None, :]], axis=1)
+    conv_out = jnp.sum(window.astype(F32) * conv_taps[None], axis=1).astype(BF16)
+    new_conv_state = window[:, 1:, :]
+    blocks = conv_out.reshape(batch_rows, recur_gate_blocks.shape[0], recur_gate_blocks.shape[1])
+
+    def gate_of(maps_of):
+        return jax.nn.sigmoid(
+            jnp.einsum("bhi,hij->bhj", blocks, maps_of, preferred_element_type=F32).reshape(
+                batch_rows, channels
+            )
+        )
+
+    recur_gate = gate_of(recur_gate_blocks)
+    input_gate = gate_of(input_gate_blocks)
+    log_decay = -decay_scale * recur_gate * decay_rate
+    new_state = jnp.exp(log_decay) * recur_state + jnp.sqrt(
+        -jnp.expm1(2.0 * log_decay)
+    ) * input_gate * conv_out.astype(F32)
+    mixer_rows = (new_state * jax.nn.gelu(gate_branch.astype(F32))).astype(BF16)
+    f = expert_down.shape[1]
+    layer_out = rest(
+        n, m, experts, mixer_rows, out_weight, tokens, ffn_gain[None, :], mask, maps,
+        dense_gate, dense_up, dense_down,
+        expert_gate.reshape(n, q, f), expert_up.reshape(n, q, f), expert_down[0],
+    )
+    return (layer_out, new_state, new_conv_state)
+
+
 def solution(mesh):
     in_specs = (
         P("ep", None),
@@ -184,6 +661,17 @@
         P(),
     )
     out_specs = (P("ep", None), P("ep", "tp"), P("ep", None, "tp"))
+    n, m = mesh.shape["ep"], mesh.shape["tp"]
+
+    def body(*args):
+        tokens, router, dense = args[0], args[12], args[17]
+        q = tokens.shape[1] // n
+        fits = n == 2 * m and n == router.shape[1] < LANES and q % (m * LANES) == 0
+        fits = fits and tokens.shape[0] % 16 == 0 and dense.shape[1] % LANES == 0
+        if fits:
+            return in_kernels(n, m, *args)
+        return on_device(*args)
+
     return jax.shard_map(
-        on_device, mesh=mesh, in_specs=in_specs, out_specs=out_specs, check_vma=False
-    )
+        body, mesh=mesh, in_specs=in_specs, out_specs=out_specs, check_vma=False
+    )

time: 398 us -> 126 us (0.32)
  waiting for transfers between devices: 308 us -> 0 us
  Pallas kernels: 0 us -> 111 us
  blocking collectives: 30.1 us -> 0 us
  matrix products: 26.9 us -> 0.42 us
  between operations: 14.4 us -> 0.83 us
  starting transfers between devices: 8.4 us -> 0 us
  local copies, waits for them, and re-layouts: 2.18 us -> 9.39 us
    all_gather x2 -> x0, waiting for transfers between devices: 129 us -> none  [the longest x1 79.5 us: on_device(): lax.all_gather(out_weight, 'ep', axis=1, tiled=True)]
    pallas_call x0 -> x2, Pallas kernels: none -> 111 us  [the longest x1 85.2 us: rest(): pl.pallas_call(functools.partial(layer_kernel, n, m, experts), out_shape=...]
    psum x2 -> x0, waiting for transfers between devices: 97 us -> none  [the longest x1 55.4 us: on_device(): total = lax.psum(partial_value.astype(jnp.bfloat16), 'tp')]
    reduce_scatter x2 -> x0, waiting for transfers between devices: 55.4 us -> none  [the longest x1 30.9 us: on_device(): lax.psum_scatter(jnp.dot(arrived, joined, preferred_element_type=jnp.floa...]
    all_to_all x2 -> x0, blocking collectives: 30.1 us -> none  [the longest x1 16 us: on_device(): lax.all_to_all(normed, 'ep', split_axis=1, concat_axis=0, tiled=True)]
    dot_general x12 -> x2, matrix products: 26.9 us -> 0.42 us  [gate_of(): jnp.einsum('bhi,hij->bhj', blocks, maps_of, preferred_element_type=F32)]
    all_to_all x2 -> x0, waiting for transfers between devices: 25.4 us -> none  [the longest x1 25.4 us: on_device(): lax.all_to_all(total.reshape(sources, items, total.shape[1]), 'ep', split...]
    all_to_all x2 -> x0, starting transfers between devices: 8.16 us -> none  [the longest x1 4.6 us: on_device(): lax.all_to_all(total.reshape(sources, items, total.shape[1]), 'ep', split...]
  transfers between devices with their start and end apart: 8 -> 0, of which waited for: 7 -> 0; matrix products, arithmetic and copies ran while one was open for 3% -> 0% of each run, Pallas kernels for 0% -> 0%
where the time goes in v1:
time: 126 us
  Pallas kernels  111 us (88%)
  local copies, waits for them, and re-layouts  9.39 us (7%)
  other arithmetic  3.89 us (3%)
    pallas_call x1, Pallas kernels, rest(): pl.pallas_call(functools.partial(layer_kernel, n, m, experts), out_shape=...  85.2 us
    pallas_call x1, Pallas kernels, project(): pl.pallas_call(functools.partial(project_kernel, n), out_shape=jax.ShapeD...  25.8 us
    unnamed x28, local copies, waits for them, and re-layouts  6.47 us

profile of v1, /device:TPU:0, one launch (start us, length us, event | category | flops | bytes accessed | tf_op | source)
XLA Modules:
  0.0 125.6 jit_solution(4235830036452716684)
XLA Ops:
  0.6 0.0 copy-start
  0.6 0.0 copy-start.1
  0.7 1.0 copy-done.1
  1.6 0.0 copy-start.2
  1.6 1.2 copy-done.2
  2.9 0.0 copy-start.3
  2.9 1.2 copy-done.3
  4.1 0.0 copy-start.4
  4.1 0.7 copy-done.4
  4.8 0.0 copy-start.5
  4.8 0.0 copy-start.8
  4.8 25.8 %project.1 = bf16[32,2048]{1,0:T(8,128)(2,1)S(1)} custom-call(bf16[32,4096]{1,0:T(8,128)(2,1)S(1)} %copy-done.1, f32[1,4096]{1,0:T(1,128)S(1)} %bitcast.18, bf16[512,1024]{1,0:T(8,128)(2,1)S(1)} %copy-done.2, bf16[512,1024]{1,0:T(8,128)(2,1)S(1)} %copy-done.3), custom_call_target="tpu_custom_call" | custom-call | tf_op jit(solution)/shard_map/project/pallas_call | solution.py:266
  30.6 0.0 copy-start.12
  30.6 0.0 copy-done.5
  30.6 0.0 copy-done.8
  30.7 0.1 multiply_reduce_fusion
  30.7 0.1 convert_element_type.24
  30.9 0.0 copy-done
  30.9 0.0 copy-start.10
  30.9 0.0 copy-start.6
  30.9 0.2 fusion.7
  31.1 0.0 copy-start.11
  31.1 0.0 copy-start.7
  31.1 0.2 copy.30
  31.3 0.1 div.13
  31.4 0.1 copy-done.12
  31.6 0.0 copy-start.9
  31.6 0.2 fusion.3
  31.8 0.2 copy.32
  31.9 0.1 div.15
  32.1 0.0 copy-done.10
  32.1 0.0 copy-done.6
  32.1 0.8 fusion.15
  32.9 0.0 copy-done.11
  32.9 0.7 fusion.19.mask
  33.6 0.0 copy-done.7
  33.6 0.5 copy.33
  34.1 0.0 copy-done.9
  34.1 2.1 %concatenate.15 = bf16[8,512,1]{2,1,0:T(8,128)(2,1)S(1)} reshape(bf16[4096]{0:T(1024)(128)(2,1)S(1)} %copy-done.9) | data formatting | bytes 16384 | tf_op jit(solution)/shard_map/concatenate | solution.py:601
  36.3 0.1 pad.2.clone
  36.3 1.6 %maximum_maximum_fusion.rb = bf16[8,512,128]{2,1,0:T(8,128)(2,1)} fusion(bf16[8,512,1]{2,1,0:T(8,128)(2,1)S(1)} %concatenate.15, bf16[8,512,8]{2,1,0:T(8,128)(2,1)S(1)} %bitcast.22, bf16[128]{0:T(256)(128)(2,1)S(1)} %pad.2.clone), kind=kLoop, calls=%fused_computation.10 | loop fusion | flops 3145728 | bytes 1122560 | tf_op jit(solution)/shard_map/concatenate | solution.py:601
  38.0 85.2 %rest.1 = bf16[32,4096]{1,0:T(8,128)(2,1)} custom-call(bf16[32,1024]{1,0:T(8,128)(2,1)} %get-tuple-element.3.mr, bf16[1024,512]{1,0:T(8,128)(2,1)} %ow.1, bf16[32,4096]{1,0:T(8,128)(2,1)} %tokens.3, f32[1,4096]{1,0:T(1,128)} %bitcast.23, bf16[32,128]{1,0:T(8,128)(2,1)} %fusion.19.mask, bf16[8,512,128]{2,1,0:T(8,128)(2,1)} %maximum_maximum_fusion.rb, ...), custom_call_target="tpu_custom_call" | custom-call | tf_op jit(solution)/shard_map/rest/pallas_call | solution.py:563
  123.2 0.7 fusion.8
  123.9 1.7 %copy.40 = bf16[32,4096]{1,0:T(8,128)(2,1)} copy(bf16[32,4096]{1,0:T(8,128)(2,1)} %rest.1) | data formatting | bytes 524288
  (4 shorter events, 0.0 us)
Async XLA Ops:
  0.6 30.2 %copy-start = (bf16[16,64,64]{2,1,0:T(8,128)(2,1)S(1)}, bf16[16,64,64]{2,1,0:T(8,128)(2,1)}, u32[]{:S(2)}) copy-start(bf16[16,64,64]{2,1,0:T(8,128)(2,1)} %param.28) | copy-start | bytes 393220
  0.6 1.0 copy-start.1
  1.6 1.2 copy-start.2
  2.9 1.2 copy-start.3
  4.1 0.7 copy-start.4
  4.8 25.8 %copy-start.5 = (bf16[32,3,1024]{2,0,1:T(8,128)(2,1)S(1)}, bf16[32,3,1024]{2,0,1:T(8,128)(2,1)}, u32[]{:S(2)}) copy-start(bf16[32,3,1024]{2,0,1:T(8,128)(2,1)} %param.23) | copy-start | bytes 589828
  4.8 25.8 %copy-start.8 = (f32[4,1024]{1,0:T(4,128)S(1)}, f32[4,1024]{1,0:T(4,128)}, u32[]{:S(2)}) copy-start(f32[4,1024]{1,0:T(4,128)} %param.27) | copy-start | bytes 49156
  30.6 1.0 copy-start.12
  30.9 1.2 copy-start.10
  30.9 1.2 copy-start.6
  31.1 1.8 %copy-start.11 = (s32[32,2]{0,1:T(2,128)S(1)}, s32[32,2]{0,1:T(2,128)}, u32[]{:S(2)}) copy-start(s32[32,2]{0,1:T(2,128)} %param.34) | copy-start | bytes 772
  31.1 2.5 %copy-start.7 = (bf16[4096,8]{0,1:T(8,128)(2,1)S(1)}, bf16[4096,8]{0,1:T(8,128)(2,1)}, u32[]{:S(2)}) copy-start(bf16[4096,8]{0,1:T(8,128)(2,1)} %param.33) | copy-start | bytes 196612
  31.6 2.5 %copy-start.9 = (bf16[4096]{0:T(1024)(128)(2,1)S(1)}, bf16[4096]{0:T(1024)(128)(2,1)}, u32[]{:S(2)}) copy-start(bf16[4096]{0:T(1024)(128)(2,1)} %param.41) | copy-start | bytes 24580

commit v2 on v1

--- a/solution.py
+++ b/solution.py
@@ -223,41 +223,52 @@
 
 
 def project_kernel(
-    n, tokens, gain, iw, gw, out, nsend, narr, psend, precv, keep, rsend, rrecv, s1, r1, s2, r2, s3, r3
+    n, tokens, gain, iw_hbm, gw_hbm, out, toks, iw, gw, lw, narr, psend, precv, keep, rsend, rrecv, s1, r1, s2, r2, s3, r3
 ):
     me, tp = lax.axis_index("ep"), lax.axis_index("tp")
     zs = n // 2
     q, ch = iw.shape
+    g = toks.shape[2]
+    loads = [
+        pltpu.make_async_copy(iw_hbm, iw, lw.at[0]),
+        pltpu.make_async_copy(gw_hbm, gw, lw.at[1]),
+    ]
+    for cp in loads:
+        cp.start()
     greet([(lax.rem(me + d, n), tp) for d in range(1, n)])
-    values = tokens[...].astype(F32)
-    inverse = lax.rsqrt(jnp.mean(values * values, axis=-1, keepdims=True) + epsilon)
-    normed = (values * inverse * gain[...]).astype(BF16)
-    for e in range(n):
-        nsend[e] = normed[:, e * q : (e + 1) * q]
+
+    def columns(e):
+        return pl.ds(pl.multiple_of(e * q, LANES), q)
+
     sends = []
     for d in range(1, n):
         to = lax.rem(me + d, n)
-        cp = rcopy(nsend.at[to], narr.at[me], s1.at[d], r1.at[d], to, tp)
+        cp = rcopy(tokens.at[:, columns(to)], narr.at[me], s1.at[d], r1.at[d], to, tp)
         cp.start()
         sends.append(cp)
-    narr[me] = nsend[me]
+    narr[me] = tokens[:, columns(me)]
+    values = tokens[...].astype(F32)
+    inverse = lax.rsqrt(jnp.mean(values * values, axis=-1, keepdims=True) + epsilon)
+    for cp in loads:
+        cp.wait()
     for d in range(1, n):
         frm = lax.rem(me - d + n, n)
         rcopy(narr.at[frm], narr.at[frm], s1.at[d], r1.at[d], frm, tp).wait_recv()
 
     def part(zz, core):
-        rows = narr[2 * zz + core]
+        rows = (narr[2 * zz + core].astype(F32) * gain[me]).astype(BF16)
         return jnp.concatenate([dot(rows, iw[...]), dot(rows, gw[...])], axis=1).astype(psend.dtype)
 
     more, finish = split_sum(
         me, tp, zs, None, psend, precv, keep, rsend, rrecv, s2, r2, s3, r3, part, lambda: None
     )
-    out[...] = finish().astype(BF16)
+    toks[...] = narr[:, :, pl.ds(pl.multiple_of(tp * g, LANES), g)]
+    out[...] = (finish() * inverse).astype(BF16)
     for cp in sends + more:
         cp.wait_send()
 
 
-def project(n, tokens, gain, iw, gw):
+def project(n, m, tokens, gain, iw, gw):
     rows, width = tokens.shape
     q, ch = iw.shape
     zs = n // 2
@@ -265,11 +276,16 @@
     dma = pltpu.SemaphoreType.DMA
     return pl.pallas_call(
         functools.partial(project_kernel, n),
-        out_shape=jax.ShapeDtypeStruct((rows, 2 * ch), BF16),
-        in_specs=[vm] * 4,
-        out_specs=vm,
+        out_shape=(
+            jax.ShapeDtypeStruct((rows, 2 * ch), BF16),
+            jax.ShapeDtypeStruct((n, rows, q // m), BF16),
+        ),
+        in_specs=[vm] * 2 + [pl.BlockSpec(memory_space=pl.ANY)] * 2,
+        out_specs=(vm, vm),
         scratch_shapes=[
-            pltpu.VMEM((n, rows, q), BF16),
+            pltpu.VMEM((q, ch), BF16),
+            pltpu.VMEM((q, ch), BF16),
+            dma((2,)),
             pltpu.VMEM((n, rows, q), BF16),
             pltpu.VMEM((zs, rows, 2 * ch), BF16),
             pltpu.VMEM((zs, rows, 2 * ch), BF16),
@@ -284,15 +300,15 @@
             dma((zs,)),
         ],
         compiler_params=pltpu.CompilerParams(
-            collective_id=0, has_side_effects=True, vmem_limit_bytes=40 * 1024 * 1024
+            collective_id=0, has_side_effects=True, vmem_limit_bytes=60 * 1024 * 1024
         ),
         name="project",
     )(tokens, gain, iw, gw)
 
 
 def layer_kernel(
-    n, m, experts, mr, ow, tokens, gain, mask, rb, dg, du, dd, eg, eu, ed, out,
-    wg, wu, wd, mall, masks, osend, orecv, full, nf, accg, accu, act,
+    n, m, experts, mr, toks, gain, mask, rb, bg, ow_hbm, dg_hbm, du_hbm, dd_hbm, eg, eu, ed, out,
+    ow, dg, du, dd, lacc, square, bacc, wg, wu, wd, mall, masks, osend, orecv, full, nf, accg, accu, act,
     psend, precv, dkeep, rsend, rrecv, dact, dall,
     ysend, yrecv, keep, xsend, xrecv, zsend, zrecv, fblk, fin,
     lw, ks, kr, as_, ar, bs, br, os_, or_, zs_, zr, xs, xr, ms, mrv,
@@ -302,15 +318,18 @@
     zs = n // 2
     z, c = me // 2, me % 2
     mate = 2 * z + 1 - c
-    rows, width = tokens.shape
+    rows, width = out.shape
     q = ow.shape[1]
     g = q // m
-    everyone = [
-        (lax.rem(me + de, n), lax.rem(tp + dt, m))
-        for de in range(n)
-        for dt in range(m)
-        if de or dt
+    peers = [(lax.rem(me + d, n), tp) for d in range(1, n)]
+    for d in range(1, m):
+        peers += [(me, lax.rem(tp + d, m)), (mate, lax.rem(tp + d, m))]
+    small = [
+        pltpu.make_async_copy(a, b, lw.at[n + 2 + k])
+        for k, (a, b) in enumerate(((ow_hbm, ow), (dg_hbm, dg), (du_hbm, du), (dd_hbm, dd)))
     ]
+    for cp in small:
+        cp.start()
     loads = [
         pltpu.make_async_copy(eg, wg, lw.at[n]),
         pltpu.make_async_copy(eu, wu, lw.at[n + 1]),
@@ -319,7 +338,7 @@
     ]
     for cp in loads:
         cp.start()
-    greet(everyone)
+    greet(peers)
     sends = []
 
     def send(*args):
@@ -357,33 +376,27 @@
             arrive(buf.at[2 * zfrom(dz) + 1 - c], r_b.at[dz])
 
     gather(mr, mall, as_, ar, bs, br)
+    for d in range(1, n):
+        send(mask, masks.at[me], ks.at[d], kr.at[d], lax.rem(me + d, n), tp)
+    masks[me] = mask[...]
+    for cp in small:
+        cp.wait()
     gathered(mall, br)
     mixed = dot(mall[...].reshape(n * rows, mr.shape[1]), ow[...]).astype(BF16)
-    for r in range(n):
-        for t in range(m):
-            osend[r, t] = mixed[r * rows : (r + 1) * rows, t * g : (t + 1) * g]
-    for de in range(n):
-        for dt in range(m):
-            if de or dt:
-                r, t = lax.rem(me + de, n), tto(dt)
-                k = de * m + dt
-                send(osend.at[r, t], orecv.at[tp, me], os_.at[k], or_.at[k], r, t)
-    orecv[tp, me] = osend[me, tp]
-    for d in range(1, n):
-        to = lax.rem(me + d, n)
-        send(mask, masks.at[me], ks.at[d], kr.at[d], to, tp)
-    masks[me] = mask[...]
-    for de in range(n):
-        for dt in range(m):
-            if de or dt:
-                k = de * m + dt
-                arrive(orecv.at[tfrom(dt), lax.rem(me - de + n, n)], or_.at[k])
-    for e in range(n):
-        total = orecv[0, e].astype(F32)
-        for t in range(1, m):
-            total += orecv[t, e].astype(F32)
-        own = tokens[:, pl.ds(pl.multiple_of(e * q + tp * g, LANES), g)].astype(F32)
-        full[tp, me, e] = (own + total).astype(BF16)
+    for t in range(m):
+        osend[t] = mixed[:, t * g : (t + 1) * g].reshape(n, rows, g)
+    for dt in range(1, m):
+        send(osend.at[tto(dt)], orecv.at[tp], os_.at[dt], or_.at[dt], me, tto(dt))
+    total = toks[...].astype(F32) + osend[tp].astype(F32)
+    accg[...] = jnp.zeros_like(accg)
+    accu[...] = jnp.zeros_like(accu)
+    lacc[...] = jnp.zeros_like(lacc)
+    square[...] = jnp.zeros_like(square)
+    bacc[...] = jnp.zeros_like(bacc)
+    for dt in range(1, m):
+        arrive(orecv.at[tfrom(dt)], or_.at[dt])
+        total += orecv[tfrom(dt)].astype(F32)
+    full[tp, me] = total.astype(BF16)
 
     def spread(slot, dz):
         for dt in range(1, m):
@@ -399,61 +412,64 @@
         slot = 2 * zfrom(dz) + c
         arrive(full.at[tp, slot], zr.at[dz])
         spread(slot, dz)
-    for dz in range(zs):
+    def relay(dz):
         slot = 2 * zfrom(dz) + c
         for dt in range(1, m):
             k = dz * m + dt
-            arrive(full.at[tfrom(dt), slot], xr.at[k])
-            send(
-                full.at[tfrom(dt), slot], full.at[tfrom(dt), slot], ms.at[k], mrv.at[k], mate, tp
-            )
-    for dz in range(zs):
+            at = full.at[tfrom(dt), slot]
+            arrive(at, xr.at[k])
+            send(at, at, ms.at[k], mrv.at[k], mate, tp)
+
+    def expert_in(dz):
         slot = 2 * zfrom(dz) + 1 - c
         for dt in range(m):
             arrive(full.at[tfrom(dt), slot], mrv.at[dz * m + dt])
 
-    @pl.loop(0, n)
-    def _(r):
-        square = jnp.zeros((rows, g), F32)
-        for t in range(m):
-            for e in range(n):
-                v = full[t, r, e].astype(F32)
-                square += v * v
-        inverse = lax.rsqrt(jnp.sum(square, axis=-1, keepdims=True) / width + epsilon)
-        for t in range(m):
-            for e in range(n):
-                at = e * q + t * g
-                nf[e, r, :, t * g : (t + 1) * g] = (
-                    full[t, r, e].astype(F32) * inverse * gain[:, at : at + g]
-                ).astype(BF16)
-
-    def expert_in(first, last):
-        @pl.loop(first, last)
-        def _(k):
-            x = nf[k].reshape(n * rows, q)
-            accg[...] += dot(x, wg[k])
-            accu[...] += dot(x, wu[k])
+        @pl.loop(0, 2)
+        def _(core):
+            e = 2 * zfrom(dz) + core
+            for t in range(m):
+                at = slice(t * g, (t + 1) * g)
+                v = full[t, e].reshape(n * rows, g).astype(F32)
+                square[...] += v * v
+                scaled = (v * gain[e, :, at]).astype(BF16)
+                bacc[...] += scaled.astype(F32) * bg[e, :, at].astype(F32)
+                nf[e, :, :, at] = scaled.reshape(n, rows, g)
+            x = nf[e].reshape(n * rows, q)
+            accg[...] += dot(x, wg[e])
+            accu[...] += dot(x, wu[e])
+            maps = rb[:, pl.ds(pl.multiple_of(e * q, LANES), q)]
+            lacc[...] += lax.dot_general(
+                x, maps, (((1,), (1,)), ((), ())), preferred_element_type=F32
+            )
+
+    loads[0].wait()
+    loads[1].wait()
+    relay(0)
+    relay(1)
+    expert_in(0)
 
     def dpart(zz, core):
         x = nf[me, 2 * zz + core]
         return jnp.concatenate([dot(x, dg[...]), dot(x, du[...])], axis=1).astype(BF16)
 
     def between():
-        accg[...] = jnp.zeros_like(accg)
-        accu[...] = jnp.zeros_like(accu)
-        loads[0].wait()
-        loads[1].wait()
-        expert_in(0, n // 4)
+        for dz in range(2, zs):
+            relay(dz)
+        expert_in(1)
 
     more, finish = split_sum(
         me, tp, zs, None, psend, precv, dkeep, rsend, rrecv, s2, r2, s3, r3, dpart, between
     )
     sends += more
-    expert_in(n // 4, n)
-    gate = accg[...]
-    act[...] = (gate * jax.nn.sigmoid(gate) * accu[...]).astype(BF16)
+    for dz in range(2, zs):
+        expert_in(dz)
+    inverse = lax.rsqrt(jnp.sum(square[...], axis=-1, keepdims=True) / width + epsilon)
+    gate = accg[...] * inverse
+    act[...] = (gate * jax.nn.sigmoid(gate) * (accu[...] * inverse)).astype(BF16)
     h = dg.shape[1]
-    both = finish()
+    square[:, 0:1] = inverse
+    both = finish() * square[pl.ds(pl.multiple_of(me * rows, rows), rows), 0:1]
     first = both[:, :h]
     dact[...] = (first * jax.nn.sigmoid(first) * both[:, h:]).astype(BF16)
     for dz in range(1, zs):
@@ -461,20 +477,16 @@
     send(dact, dall.at[me], es.at[0], er.at[0], mate, tp)
     dall[me] = dact[...]
 
-    logits = dot(nf[0].reshape(n * rows, q), rb[0])
-    for k in range(1, n):
-        logits += dot(nf[k].reshape(n * rows, q), rb[k])
+    logits = lacc[...] * inverse
     for d in range(1, n):
         arrive(masks.at[lax.rem(me - d + n, n)], kr.at[d])
-    chosen = masks[...].reshape(n * rows, LANES).astype(F32)
+    chosen = masks[...].reshape(n * rows, LANES)[:, :experts].astype(F32)
     named = logits * chosen
     other = jnp.sum(named, axis=-1, keepdims=True) - named
     weight = (jax.nn.sigmoid(logits - other) * chosen).astype(BF16).astype(F32)
-    lane = lax.broadcasted_iota(jnp.int32, (n * rows, LANES), 1)
+    lane = lax.broadcasted_iota(jnp.int32, (n * rows, experts), 1)
     weight = jnp.sum(jnp.where(lane == me, weight, 0.0), axis=-1, keepdims=True)
-    branch = jnp.sum(
-        jnp.where(lane == experts, jax.nn.sigmoid(logits), 0.0), axis=-1, keepdims=True
-    )
+    branch = jax.nn.sigmoid(jnp.sum(bacc[...], axis=-1, keepdims=True) * inverse)
 
     for cp in loads[2:]:
         cp.wait()
@@ -526,7 +538,7 @@
         total += zrecv[zfrom(dz)].astype(F32)
     chunk = 2 * tp + c
     for core in range(2):
-        resid = jnp.concatenate([full[t, 2 * z + core, chunk] for t in range(m)], axis=1)
+        resid = jnp.concatenate([full[t, chunk, 2 * z + core] for t in range(m)], axis=1)
         fblk[core] = (resid.astype(F32) + total[core * rows : (core + 1) * rows]).astype(BF16)
     for dc in range(2):
         for dt in range(m):
@@ -548,8 +560,8 @@
         rcopy(xrecv.at[dt], xrecv.at[dt], hs.at[dt], hr.at[dt], mate, tp).wait_send()
 
 
-def rest(n, m, experts, mr, ow, tokens, gain, mask, rb, dg, du, dd, eg, eu, ed):
-    rows, width = tokens.shape
+def rest(n, m, experts, mr, toks, gain, mask, rb, bg, ow, dg, du, dd, eg, eu, ed):
+    rows, width = mr.shape[0], ow.shape[1] * n
     ch, q = ow.shape
     h, f = dg.shape[1], ed.shape[0]
     g, zs, b = q // m, n // 2, n * rows
@@ -563,12 +575,14 @@
     return pl.pallas_call(
         functools.partial(layer_kernel, n, m, experts),
         out_shape=jax.ShapeDtypeStruct((rows, width), BF16),
-        in_specs=[vm] * 9 + [hbm] * 3,
+        in_specs=[vm] * 6 + [hbm] * 7,
         out_specs=vm,
         scratch_shapes=[
+            v((ch, q), BF16), v((q, h), BF16), v((q, h), BF16), v((h, q), BF16),
+            v((b, experts), F32), v((b, g), F32), v((b, g), F32),
             v((n, q, f), BF16), v((n, q, f), BF16), v((n, f, q), BF16),
             v((n, rows, ch), BF16), v((n, rows, LANES), BF16),
-            v((n, m, rows, g), BF16), v((m, n, rows, g), BF16),
+            v((m, n, rows, g), BF16), v((m, n, rows, g), BF16),
             v((m, n, n, rows, g), BF16), v((n, n, rows, q), BF16),
             v((b, f), F32), v((b, f), F32), v((b, f), BF16),
             v((zs, rows, 2 * h), BF16), v((zs, rows, 2 * h), BF16), v((zs, rows, 2 * h), F32),
@@ -578,13 +592,13 @@
             v((m, b, q), BF16), v((m, b, q), BF16),
             v((zs, 2 * rows, q), BF16), v((zs, 2 * rows, q), BF16),
             v((2, rows, q), BF16), v((n, rows, q), BF16),
-            pltpu.SemaphoreType.DMA((n + 2,)),
-        ] + pairs(n, zs, zs, n * m, zs, zs * m, zs * m, zs, zs, zs, zs, m, m, zs, 2 * m),
+            pltpu.SemaphoreType.DMA((n + 6,)),
+        ] + pairs(n, zs, zs, m, zs, zs * m, zs * m, zs, zs, zs, zs, m, m, zs, 2 * m),
         compiler_params=pltpu.CompilerParams(
             collective_id=1, has_side_effects=True, vmem_limit_bytes=58 * 1024 * 1024
         ),
         name="rest",
-    )(mr, ow, tokens, gain, mask, rb, dg, du, dd, eg, eu, ed)
+    )(mr, toks, gain, mask, rb, bg, ow, dg, du, dd, eg, eu, ed)
 
 
 def in_kernels(
@@ -598,15 +612,7 @@
     q = width // n
     lanes = lax.broadcasted_iota(jnp.int32, (batch_rows, LANES), 1)
     mask = ((routes[:, 0:1] == lanes) | (routes[:, 1:2] == lanes)).astype(BF16)
-    maps = jnp.concatenate(
-        [
-            router_weight,
-            branch_gate[:, None],
-            jnp.zeros((width, LANES - experts - 1), BF16),
-        ],
-        axis=1,
-    ).reshape(n, q, LANES)
-    summed = project(n, tokens, mix_gain[None, :], in_weight, gate_weight)
+    summed, toks = project(n, m, tokens, mix_gain.reshape(n, 1, q), in_weight, gate_weight)
     x_branch, gate_branch = summed[:, :channels], summed[:, channels:]
     window = jnp.concatenate([conv_state, x_branch[:, None, :]], axis=1)
     conv_out = jnp.sum(window.astype(F32) * conv_taps[None], axis=1).astype(BF16)
@@ -629,8 +635,8 @@
     mixer_rows = (new_state * jax.nn.gelu(gate_branch.astype(F32))).astype(BF16)
     f = expert_down.shape[1]
     layer_out = rest(
-        n, m, experts, mixer_rows, out_weight, tokens, ffn_gain[None, :], mask, maps,
-        dense_gate, dense_up, dense_down,
+        n, m, experts, mixer_rows, toks, ffn_gain.reshape(n, 1, q), mask,
+        router_weight.T, branch_gate.reshape(n, 1, q), out_weight, dense_gate, dense_up, dense_down,
         expert_gate.reshape(n, q, f), expert_up.reshape(n, q, f), expert_down[0],
     )
     return (layer_out, new_state, new_conv_state)

time: 126 us -> 111 us (0.88)
  Pallas kernels: 111 us -> 102 us
  local copies, waits for them, and re-layouts: 9.39 us -> 3.94 us
    pallas_call x1, Pallas kernels: 85.2 us -> 75.1 us  [rest(): pl.pallas_call(functools.partial(layer_kernel, n, m, experts), out_shape=...]
    unnamed x28 -> x17, local copies, waits for them, and re-layouts: 6.47 us -> 1.71 us
    concatenate x2 -> x0, local copies, waits for them, and re-layouts: 2.2 us -> none  [in_kernels(): jnp.concatenate([router_weight, branch_gate[:, None], jnp.zeros((width, L...]
    concatenate x1 -> x0, other arithmetic: 1.62 us -> none  [in_kernels(): jnp.concatenate([router_weight, branch_gate[:, None], jnp.zeros((width, L...]
    pallas_call x1, Pallas kernels: 25.8 us -> 27.4 us  [project(): pl.pallas_call(functools.partial(project_kernel, n), out_shape=(jax.Shape...]
where the time goes in v2:
time: 111 us
  Pallas kernels  102 us (92%)
  local copies, waits for them, and re-layouts  3.94 us (4%)
  other arithmetic  3.19 us (3%)
    pallas_call x1, Pallas kernels, rest(): pl.pallas_call(functools.partial(layer_kernel, n, m, experts), out_shape=...  75.1 us
    pallas_call x1, Pallas kernels, project(): pl.pallas_call(functools.partial(project_kernel, n), out_shape=(jax.Shape...  27.4 us

profile of v2, /device:TPU:0, one launch (start us, length us, event | category | flops | bytes accessed | tf_op | source)
XLA Modules:
  0.0 110.8 jit_solution(11902669801563353128)
XLA Ops:
  0.6 0.0 copy-start
  0.6 0.0 copy-start.7
  0.7 0.0 copy-start.5
  0.7 0.0 copy-start.2
  0.7 0.0 copy-start.6
  0.7 0.0 copy-start.4
  0.7 27.4 %project.1 = (bf16[32,2048]{1,0:T(8,128)(2,1)}, bf16[8,32,128]{2,1,0:T(8,128)(2,1)}) custom-call(bf16[32,4096]{1,0:T(8,128)(2,1)} %tokens.1, f32[8,1,512]{2,1,0:T(1,128)} %bitcast.22, bf16[512,1024]{1,0:T(8,128)(2,1)} %iw_hbm.1, bf16[512,1024]{1,0:T(8,128)(2,1)} %gw_hbm.1), custom_call_target="tpu_custom_call" | custom-call | tf_op jit(solution)/shard_map/project/pallas_call | solution.py:277
  28.1 0.0 copy-start.3
  28.1 0.9 slice_bitcast_fusion
  29.0 1.0 multiply_reduce_fusion
  30.0 0.1 convert_element_type.24
  30.1 0.0 copy-done
  30.1 0.2 fusion.7
  30.3 0.2 copy.29
  30.5 0.1 div.13
  30.6 0.0 copy-done.7
  30.6 0.2 fusion.3
  30.9 0.2 copy.31
  31.0 0.1 div.15
  31.2 0.0 copy-done.5
  31.2 0.0 copy-done.2
  31.2 0.0 copy-done.3
  31.2 0.8 fusion.15
  32.0 0.0 copy-done.6
  32.0 0.7 fusion.19.mask
  32.7 0.0 copy-done.4
  32.7 0.6 reshape.45.bg
  33.3 0.0 copy-start.1
  33.3 75.1 %rest.1 = bf16[32,4096]{1,0:T(8,128)(2,1)} custom-call(bf16[32,1024]{1,0:T(8,128)(2,1)} %get-tuple-element.7.mr, bf16[8,32,128]{2,1,0:T(8,128)(2,1)} %get-tuple-element.6.toks, f32[8,1,512]{2,1,0:T(1,128)} %bitcast.23, bf16[32,128]{1,0:T(8,128)(2,1)} %fusion.19.mask, bf16[8,4096]{1,0:T(8,128)(2,1)} %bitcast.21, bf16[8,1,512]{2,1,0:T(2,128)(2,1)} %reshape.45.bg, ...), custom_call_target="tpu_custom_call" | custom-call | tf_op jit(solution)/shard_map/rest/pallas_call | solution.py:575
  108.5 0.0 copy-done.1
  108.5 0.7 fusion.8
  109.2 1.7 %copy.38 = bf16[32,4096]{1,0:T(8,128)(2,1)} copy(bf16[32,4096]{1,0:T(8,128)(2,1)} %rest.1) | data formatting | bytes 524288
  (2 shorter events, 0.0 us)
Async XLA Ops:
  0.6 29.5 %copy-start = (bf16[16,64,64]{2,1,0:T(8,128)(2,1)S(1)}, bf16[16,64,64]{2,1,0:T(8,128)(2,1)}, u32[]{:S(2)}) copy-start(bf16[16,64,64]{2,1,0:T(8,128)(2,1)} %param.28) | copy-start | bytes 393220
  0.6 30.0 %copy-start.7 = (bf16[16,64,64]{2,1,0:T(8,128)(2,1)S(1)}, bf16[16,64,64]{2,1,0:T(8,128)(2,1)}, u32[]{:S(2)}) copy-start(bf16[16,64,64]{2,1,0:T(8,128)(2,1)} %param.29) | copy-start | bytes 393220
  0.7 30.5 %copy-start.5 = (f32[1024]{0:T(1024)S(1)}, f32[1024]{0:T(1024)}, u32[]{:S(2)}) copy-start(f32[1024]{0:T(1024)} %param.30) | copy-start | bytes 12292
  0.7 30.5 %copy-start.2 = (f32[32,1024]{1,0:T(8,128)S(1)}, f32[32,1024]{1,0:T(8,128)}, u32[]{:S(2)}) copy-start(f32[32,1024]{1,0:T(8,128)} %param.22) | copy-start | bytes 393220
  0.7 31.4 %copy-start.6 = (s32[32,2]{0,1:T(2,128)S(1)}, s32[32,2]{0,1:T(2,128)}, u32[]{:S(2)}) copy-start(s32[32,2]{0,1:T(2,128)} %param.34) | copy-start | bytes 772
  0.7 32.0 %copy-start.4 = (bf16[4096]{0:T(1024)(128)(2,1)S(1)}, bf16[4096]{0:T(1024)(128)(2,1)}, u32[]{:S(2)}) copy-start(bf16[4096]{0:T(1024)(128)(2,1)} %param.41) | copy-start | bytes 24580
  28.1 3.1 %copy-start.3 = (bf16[32,2048]{1,0:T(8,128)(2,1)S(1)}, bf16[32,2048]{1,0:T(8,128)(2,1)}, u32[]{:S(2)}) copy-start(bf16[32,2048]{1,0:T(8,128)(2,1)} %get-tuple-element.5) | copy-start | bytes 393220
  33.3 75.1 %copy-start.1 = (bf16[32,3,1024]{2,0,1:T(8,128)(2,1)S(1)}, bf16[32,3,1024]{2,0,1:T(8,128)(2,1)}, u32[]{:S(2)}) copy-start(bf16[32,3,1024]{2,0,1:T(8,128)(2,1)} %param.23) | copy-start | bytes 589828
